TPU v7x, 32 devices: a whole 2x2x4 slice. The times are simulated.
32 devices in a mesh: sp: 4 (over x, core), tp: 8 (over z, y).
Axes of the slice: x: 2, y: 2, z: 4, core: 2. Of those that a mesh axis runs over, the one named last changes fastest.
Arguments:
- latents: bfloat16 [1024, 2048], P(('sp', 'tp')), may hold values from -6 to 6
- context: bfloat16 [256, 2048], P('sp'), may hold values from -6 to 6
- condition: float32 [2048], P('sp'), may hold values from -12 to 12
- context_condition: float32 [2048], P('sp'), may hold values from -12 to 12
- norm_gain: float32 [2048], replicated, may hold values from 0.1 to 1.9
- shift_weight: bfloat16 [2048, 2048], P('sp', 'tp'), may hold values from -0.09375 to 0.09375
- scale_weight: bfloat16 [2048, 2048], P('sp', 'tp'), may hold values from -0.09375 to 0.09375
- gate_weight: bfloat16 [2048, 2048], P('sp', 'tp'), may hold values from -0.125 to 0.125
- query_weight: bfloat16 [2048, 1024], P(None, 'tp'), may hold values from -0.125 to 0.125
- key_weight: bfloat16 [2048, 1024], P(None, 'tp'), may hold values from -0.125 to 0.125
- value_weight: bfloat16 [2048, 1024], P(None, 'tp'), may hold values from -0.125 to 0.125
- subtract_share: float32 [8], P('tp'), may hold values from 0.3 to 0.8
- head_gain: float32 [128], replicated, may hold values from 0.1 to 1.9
- output_weight: bfloat16 [1024, 2048], P('tp'), may hold values from -0.1875 to 0.1875
Outputs:
- updated: bfloat16 [1024, 2048], P(('sp', 'tp'))
All inputs are finite; a program needn't handle non-finite values.
Results may differ from a plain program's by a relative error of at most 0.013.
Values may be sent and summed in bfloat16 or wider, within the bound.
A program may use at most 64 MiB of HBM per device.

v0:
```python
import functools
import math

import jax
import jax.numpy as jnp
from jax import lax
from jax.experimental import pallas as pl
from jax.experimental.pallas import tpu as pltpu
from jax.sharding import PartitionSpec as P

HEAD = 64
VALUE = 128
GRID_W = 64


norm_eps = 1e-06
head_eps = 1e-05
rope_theta = 10000.0
head_scale = 0.8


def rotary_tables(positions):
    quarter = HEAD // 4
    inverse = rope_theta ** (-2.0 * jnp.arange(quarter, dtype=jnp.float32) / (HEAD // 2))
    row_angle = (positions // GRID_W).astype(jnp.float32)[:, None] * inverse[None, :]
    column_angle = (positions % GRID_W).astype(jnp.float32)[:, None] * inverse[None, :]
    angles = jnp.concatenate([row_angle, row_angle, column_angle, column_angle], axis=-1)
    return (jnp.cos(angles), jnp.sin(angles))


def rotate(vectors, cosine, sine_table):
    quarter = HEAD // 4
    pieces = vectors.reshape(vectors.shape[:-1] + (2, 2, quarter))
    turned = jnp.concatenate([-pieces[..., 1:, :], pieces[..., :1, :]], axis=-2).reshape(
        vectors.shape
    )
    return vectors * cosine[:, None, :] + turned * sine_table[:, None, :]


def modulate(token_rows, gain_row, shift_row, scale_row):
    widened = token_rows.astype(jnp.float32)
    normed = widened * lax.rsqrt(jnp.mean(widened * widened, axis=-1, keepdims=True) + norm_eps)
    return (normed * gain_row * (1.0 + scale_row) + shift_row).astype(jnp.bfloat16)


def shards(
    latents,
    context,
    condition,
    context_condition,
    norm_gain,
    shift_weight,
    scale_weight,
    gate_weight,
    query_weight,
    key_weight,
    value_weight,
    subtract_share,
    head_gain,
    output_weight,
):
    activated = jax.nn.silu(jnp.stack([condition, context_condition])).astype(jnp.bfloat16)
    partial_terms = jnp.stack(
        [
            jnp.dot(activated, matrix, preferred_element_type=jnp.float32)
            for matrix in (shift_weight, scale_weight, gate_weight)
        ]
    )
    summed = lax.psum(partial_terms, "sp")
    full_terms = lax.all_gather(summed, "tp", axis=2, tiled=True)
    shift_terms, scale_terms, gate_terms = (full_terms[0], full_terms[1], full_terms[2])
    pair_weight = jnp.concatenate([key_weight, value_weight], axis=1)
    joined = jnp.concatenate([query_weight, pair_weight], axis=1)
    projected = jnp.dot(
        modulate(
            lax.all_gather(latents, "tp", axis=0, tiled=True),
            norm_gain,
            shift_terms[0],
            scale_terms[0],
        ),
        joined,
        preferred_element_type=jnp.float32,
    )
    local_count = projected.shape[0]
    positions = lax.axis_index("sp") * local_count + jnp.arange(local_count, dtype=jnp.int32)
    cosine, sine_table = rotary_tables(positions)
    queries = rotate(projected[:, :VALUE].reshape(local_count, 2, HEAD), cosine, sine_table)
    queries = queries.reshape(local_count, VALUE).astype(jnp.bfloat16)
    latent_keys = rotate(
        projected[:, VALUE : 2 * VALUE].reshape(local_count, 2, HEAD), cosine, sine_table
    )
    latent_keys = latent_keys.reshape(local_count, VALUE).astype(jnp.bfloat16)
    latent_pairs = jnp.concatenate(
        [latent_keys, projected[:, 2 * VALUE :].astype(jnp.bfloat16)], axis=1
    )
    context_mod = modulate(context, norm_gain, shift_terms[1], scale_terms[1])
    context_pairs = jnp.dot(context_mod, pair_weight, preferred_element_type=jnp.float32).astype(
        jnp.bfloat16
    )
    sent_pairs = jnp.concatenate([latent_pairs, context_pairs], axis=0)
    arrived = lax.all_gather(sent_pairs, "sp", axis=0, tiled=True)
    updated_carry = []
    for which_map in range(2):
        offset = which_map * HEAD
        scores = jnp.einsum(
            "qd,kd->qk",
            queries[:, offset : offset + HEAD],
            arrived[:, offset : offset + HEAD],
            preferred_element_type=jnp.float32,
        ) * HEAD ** (-0.5)
        powers = jnp.exp(scores)
        updated_carry.append(
            jnp.dot(
                powers.astype(jnp.bfloat16), arrived[:, VALUE:], preferred_element_type=jnp.float32
            )
        )
        updated_carry.append(jnp.sum(powers, axis=1, keepdims=True))
    first_sum, first_total, second_sum, second_total = tuple(updated_carry)
    share_value = subtract_share[0]
    difference = first_sum / first_total - share_value * (second_sum / second_total)
    normed = difference * lax.rsqrt(
        jnp.mean(difference * difference, axis=1, keepdims=True) + head_eps
    )
    head_output = (normed * head_gain * head_scale).astype(jnp.bfloat16)
    branch = lax.psum_scatter(
        jnp.dot(head_output, output_weight, preferred_element_type=jnp.float32),
        "tp",
        scatter_dimension=0,
        tiled=True,
    )
    return (latents.astype(jnp.float32) + gate_terms[0] * branch).astype(jnp.bfloat16)


MESH = pl.DeviceIdType.MESH
CHUNKS = 4
WEIGHT_CHUNKS = 2
FAR_PIECES = 2


def fused_kernel(
    lat_ref, ctx_ref, cond_ref, ccond_ref, gain_ref, shift_hbm, scale_hbm, gate_hbm,
    wq_hbm, wk_hbm, wv_hbm, share_ref, hgain_ref, wo_hbm, out_ref,
    lat, mod, cmod, wqkv, wo, part, terms, tables, queries, kv, ho_send, ho,
    shift_ref, scale_ref, gate_ref, far_send, far_recv,
    load_sem, lat_ss, lat_rs, lat_yss, lat_yrs, part_ss, part_rs, term_ss, term_rs,
    kv_ss, kv_rs, ckv_ss, ckv_rs, ho_ss, ho_rs, hx_ss, hx_rs, wo_ss, wo_rs, wo_mrs, wo_yss, wo_tss, wo_trs, far_ss, far_rs,
    *, S, T,
):
    f32, bf16 = jnp.float32, jnp.bfloat16
    rows, D = lat_ref.shape
    crows = ctx_ref.shape[0]
    count = rows * T
    width = D // T
    quarter_cols = D // S
    Z = T // 2
    i = lax.axis_index("sp")
    t = lax.axis_index("tp")
    z = lax.div(t, 2)
    y = lax.rem(t, 2)
    mate = t + 1 - 2 * y
    even_layer = lax.rem(z, 2) == 0
    paired = t + 2 - 4 * lax.rem(z, 2)
    twin = i + 1 - 2 * lax.rem(i, 2)
    across = lax.rem(i + 2, S)
    twin_across = lax.rem(twin + 2, S)
    core = lax.rem(i, 2)
    side = lax.div(i, 2)
    half = D // 2
    pending = []
    late = []

    def when(cond, action):
        if cond is None:
            action()
        else:
            pl.when(cond)(action)

    def copy(src, dst, ss, rs, sp, tp):
        return pltpu.make_async_remote_copy(
            src_ref=src, dst_ref=dst, send_sem=ss, recv_sem=rs,
            device_id={"sp": sp, "tp": tp}, device_id_type=MESH,
        )

    def send(cond, src, dst, ss, rs, sp, tp, tracked=True):
        made = copy(src, dst, ss, rs, sp, tp)

        def go():
            made.start()

        when(cond, go)
        if tracked:
            pending.append((cond, made))

    def drain():
        for cond, made in pending:
            def finish(made=made):
                made.wait_send()

            when(cond, finish)
        pending.clear()

    def sent_all(view, ss):
        copy(view, view, ss, ss, twin, t).wait_send()

    def arrived(dst, ss, rs):
        copy(dst, dst, ss, rs, twin, t).wait_recv()

    loads = [
        pltpu.make_async_copy(wq_hbm, wqkv.at[:, pl.ds(0, VALUE)], load_sem.at[0]),
        pltpu.make_async_copy(wk_hbm, wqkv.at[:, pl.ds(VALUE, VALUE)], load_sem.at[1]),
        pltpu.make_async_copy(wv_hbm, wqkv.at[:, pl.ds(2 * VALUE, VALUE)], load_sem.at[2]),
        pltpu.make_async_copy(
            wo_hbm.at[:, pl.ds(pl.multiple_of(side * half, half), half)],
            wo.at[pl.ds(t * VALUE, VALUE), :],
            load_sem.at[3],
        ),
        pltpu.make_async_copy(shift_hbm, shift_ref, load_sem.at[4]),
        pltpu.make_async_copy(scale_hbm, scale_ref, load_sem.at[5]),
        pltpu.make_async_copy(gate_hbm, gate_ref, load_sem.at[6]),
    ]

    barrier = pltpu.get_barrier_semaphore()
    for k in range(1, S):
        pl.semaphore_signal(
            barrier, inc=1, device_id={"sp": lax.rem(i + k, S), "tp": t}, device_id_type=MESH
        )
    for k in range(1, T):
        pl.semaphore_signal(
            barrier, inc=1, device_id={"sp": i, "tp": lax.rem(t + k, T)}, device_id_type=MESH
        )
        pl.semaphore_signal(
            barrier, inc=1, device_id={"sp": across, "tp": lax.rem(t + k, T)}, device_id_type=MESH
        )
    for load in loads[4:] + loads[:4]:
        load.start()
    pl.semaphore_wait(barrier, S + 2 * T - 3)

    step = D // CHUNKS

    def lat_piece(block, c):
        return lat.at[pl.ds(block * rows, rows), pl.ds(c * step, step)]

    for c in range(CHUNKS):
        own = lat_ref.at[:, pl.ds(c * step, step)]
        dst = lat_piece(t, c)
        send(z < Z - 1, own, dst, lat_ss.at[c, z], lat_rs.at[c, z], i, t + 2)
        send(z > 0, own, dst, lat_ss.at[c, Z], lat_rs.at[c, z], i, t - 2)
        rs = lat_rs.at[c, Z] if c >= CHUNKS // 2 else lat_yrs.at[0]
        send(None, own, dst, lat_yss.at[0], rs, i, mate, False)

    def lat_stage(d):
        for c in range(CHUNKS):
            for sign in (-1, 1):
                block = t + 2 * d * sign
                here = z - d >= 0 if sign < 0 else z + d < Z
                onward = jnp.logical_and(here, z < Z - 1 if sign < 0 else z > 0)
                piece = lat_piece(block, c)
                layer = z + d * sign
                rs = lat_rs.at[c, layer]

                def come(piece=piece, rs=rs):
                    arrived(piece, lat_yss.at[0], rs)

                when(here, come)
                send(onward, piece, piece, lat_ss.at[c, layer], rs, i, t - 2 * sign)
                over = here
                if d == 1 and c >= CHUNKS // 2:
                    over = jnp.logical_and(here, even_layer if sign < 0 else jnp.logical_not(even_layer))
                send(over, piece, piece, lat_yss.at[0], lat_yrs.at[0], i, mate, False)

    def lat_cross():
        for c in range(CHUNKS // 2, CHUNKS):
            piece = lat_piece(mate, c)
            arrived(piece, lat_yss.at[0], lat_rs.at[c, Z])
            send(None, piece, piece, lat_ss.at[c, Z + 1], lat_yrs.at[0], i, paired)

    def silu(v):
        return v / (1.0 + jnp.exp(-v))

    depth = cond_ref.shape[1]
    line = lax.broadcasted_iota(jnp.int32, (8, depth), 0)
    act0 = jnp.broadcast_to(silu(cond_ref[...]), (8, depth))
    act1 = jnp.broadcast_to(silu(ccond_ref[...]), (8, depth))

    def two_lines(first, matrix_ref, with_second):
        left = jnp.where(line == first, act0, 0.0)
        if with_second:
            left = jnp.where(line == first + 1, act1, left)
        return jnp.dot(left.astype(bf16), matrix_ref[...], preferred_element_type=f32)

    for load in loads[4:]:
        load.wait()
    part[pl.ds(i, 1)] = (
        two_lines(0, shift_ref, True) + two_lines(2, scale_ref, True) + two_lines(4, gate_ref, False)
    )[None]
    for k in range(1, S):
        send(None, part.at[i], part.at[i], part_ss.at[0], part_rs.at[0], lax.rem(i + k, S), t, False)

    lat_stage(1)
    lat_cross()

    arrived(part.at[pl.ds(0, S - 1)], part_ss.at[0], part_rs.at[0])
    total = part[0]
    for k in range(1, S):
        total = total + part[k]
    terms[pl.ds(t, 1)] = total[None]
    for k in range(1, T):
        send(
            None, terms.at[t], terms.at[t], term_ss.at[0], term_rs.at[0], i, lax.rem(t + k, T), False
        )

    lane = lax.broadcasted_iota(jnp.int32, (count, VALUE), 1)
    place = i * count + lax.broadcasted_iota(jnp.int32, (count, VALUE), 0)
    spot = lax.rem(lane, HEAD)
    quarter = HEAD // 4
    power = lax.rem(spot, quarter).astype(f32) * (-2.0 / (HEAD // 2))
    inverse = jnp.exp(power * math.log(rope_theta))
    along = jnp.where(spot < HEAD // 2, lax.div(place, GRID_W), lax.rem(place, GRID_W))
    angle = along.astype(f32) * inverse
    even = lax.rem(lax.div(spot, quarter), 2) == 0
    tables[0] = jnp.cos(angle)
    tables[1] = jnp.sin(angle)

    weight_step = VALUE // WEIGHT_CHUNKS

    def wo_piece(block, share, w):
        return wo.at[
            pl.ds(block * VALUE + w * weight_step, weight_step),
            pl.ds(pl.multiple_of(share * quarter_cols, quarter_cols), quarter_cols),
        ]

    def wo_arrive(cond, block, rs, w):
        def come():
            arrived(wo_piece(block, core, w), wo_yss.at[0], rs)

        when(cond, come)

    def wo_send(cond, block, ss, rs, w, sp, tp, tracked=True):
        piece = wo_piece(block, core, w)
        send(cond, piece, piece, ss, rs, sp, tp, tracked)
        if tracked:
            late.append(pending.pop())

    def wo_twin(cond, block, w):
        wo_send(cond, block, wo_tss.at[0], wo_trs.at[0], w, twin, t, False)

    def wo_stage(d):
        for w in range(WEIGHT_CHUNKS):
            for sign in (-1, 1):
                layer = z + d * sign
                block = t + 2 * d * sign
                here = z - d >= 0 if sign < 0 else z + d < Z
                onward = jnp.logical_and(here, z < Z - 1 if sign < 0 else z > 0)
                wo_arrive(here, block, wo_rs.at[w, layer], w)
                wo_send(onward, block, wo_ss.at[w, layer], wo_rs.at[w, layer], w, i, t - 2 * sign)
                over = here
                if d == 1 and w >= WEIGHT_CHUNKS // 2:
                    over = jnp.logical_and(here, even_layer if sign < 0 else jnp.logical_not(even_layer))
                wo_send(over, block, wo_yss.at[0], wo_mrs.at[w, layer], w, i, mate, False)
                wo_twin(here, block, w)

    def wo_mate(d):
        for w in range(WEIGHT_CHUNKS):
            for sign in (-1, 1) if d else (1,):
                layer = z + d * sign
                block = mate + 2 * d * sign
                here = None if not d else (z - d >= 0 if sign < 0 else z + d < Z)
                wo_arrive(here, block, wo_mrs.at[w, layer], w)
                if not d and w >= WEIGHT_CHUNKS // 2:
                    wo_send(None, block, wo_ss.at[w, Z + 1], wo_mrs.at[w, z], w, i, paired)
                wo_twin(here, block, w)

    loads[3].wait()
    for d in range(2, Z):
        lat_stage(d)
        if d == 2:
            for w in range(WEIGHT_CHUNKS):
                wo_send(z < Z - 1, t, wo_ss.at[w, z], wo_rs.at[w, z], w, i, t + 2)
                wo_send(z > 0, t, wo_ss.at[w, Z], wo_rs.at[w, z], w, i, t - 2)
    for w in range(WEIGHT_CHUNKS):
        wo_send(None, t, wo_yss.at[0], wo_mrs.at[w, z], w, i, mate, False)

    arrived(terms.at[pl.ds(0, T - 1)], term_ss.at[0], term_rs.at[0])

    def modulate_into(dst, src, first, n, which):
        wide = src[...].astype(f32)
        factor = lax.rsqrt(jnp.mean(wide * wide, axis=-1, keepdims=True) + norm_eps)
        for j in range(T):
            cols = slice(j * width, (j + 1) * width)
            mult = gain_ref[:, cols] * (1.0 + terms[j, 2 + which : 3 + which, :])
            shifted = wide[:, cols] * factor * mult + terms[j, which : which + 1, :]
            dst[pl.ds(first, n), cols] = shifted.astype(bf16)

    for load in loads[:3]:
        load.wait()
    modulate_into(cmod, ctx_ref, 0, crows, 1)
    kv[pl.ds(i, 1), pl.ds(count, crows), :] = jnp.dot(
        cmod[...], wqkv[:, VALUE:], preferred_element_type=f32
    ).astype(bf16)[None]

    def ckv_piece(s):
        return kv.at[s, pl.ds(count, crows), :]

    def kv_piece(s):
        return kv.at[s, pl.ds(0, count), :]

    send(None, ckv_piece(i), ckv_piece(i), ckv_ss.at[0], ckv_rs.at[i], across, t)
    send(None, ckv_piece(i), ckv_piece(i), ckv_ss.at[1], ckv_rs.at[i], twin, t)

    over_rows = Z * rows - rows // 2
    arrived(lat.at[pl.ds(0, over_rows), :], lat_yss.at[0], lat_yrs.at[0])
    lat[pl.ds(t * rows, rows), :] = lat_ref[...]
    modulate_into(mod, lat, 0, count, 0)
    projected = jnp.dot(mod[...], wqkv[...], preferred_element_type=f32)

    def rotated(u):
        turned = jnp.where(even, -pltpu.roll(u, VALUE - quarter, 1), pltpu.roll(u, quarter, 1))
        return u * tables[0] + turned * tables[1]

    kv[pl.ds(i, 1), pl.ds(0, count), pl.ds(0, VALUE)] = (
        rotated(projected[:, VALUE : 2 * VALUE]).astype(bf16)[None]
    )
    kv[pl.ds(i, 1), pl.ds(0, count), pl.ds(VALUE, VALUE)] = (
        projected[:, 2 * VALUE :].astype(bf16)[None]
    )
    send(None, kv_piece(i), kv_piece(i), kv_ss.at[0], kv_rs.at[i], across, t)
    send(None, kv_piece(i), kv_piece(i), kv_ss.at[1], kv_rs.at[i], twin, t)
    arrived(ckv_piece(across), ckv_ss.at[2], ckv_rs.at[across])
    send(None, ckv_piece(across), ckv_piece(across), ckv_ss.at[2], ckv_rs.at[across], twin, t)
    query = rotated(projected[:, :VALUE]).astype(bf16) * jnp.asarray(HEAD ** (-0.5), bf16)
    first_half = lane < HEAD
    zero = jnp.zeros_like(query)
    queries[0:count, :] = jnp.where(first_half, query, zero)
    queries[count:, :] = jnp.where(first_half, zero, query)

    ones = jnp.ones((count + crows, VALUE), bf16)

    def attend(slot):
        rows_kv = kv[slot]
        scores = lax.dot_general(
            queries[...], rows_kv[:, :VALUE], (((1,), (1,)), ((), ())), preferred_element_type=f32
        )
        return jnp.dot(
            jnp.exp(scores).astype(bf16),
            jnp.concatenate([rows_kv[:, VALUE:], ones], axis=1),
            preferred_element_type=f32,
        )

    sums = attend(i)
    wo_stage(1)
    wo_mate(0)
    arrived(kv_piece(twin), kv_ss.at[2], kv_rs.at[twin])
    arrived(ckv_piece(twin), ckv_ss.at[2], ckv_rs.at[twin])
    sums = sums + attend(twin)
    arrived(kv_piece(across), kv_ss.at[2], kv_rs.at[across])
    send(None, kv_piece(across), kv_piece(across), kv_ss.at[2], kv_rs.at[across], twin, t)
    wo_stage(2)
    sums = sums + attend(across)
    arrived(kv_piece(twin_across), kv_ss.at[2], kv_rs.at[twin_across])
    arrived(ckv_piece(twin_across), ckv_ss.at[2], ckv_rs.at[twin_across])
    sums = sums + attend(twin_across)
    ratio = sums[:, :VALUE] / sums[:, VALUE:]
    difference = ratio[:count] - share_ref[0] * ratio[count:]
    normed = difference * lax.rsqrt(
        jnp.mean(difference * difference, axis=1, keepdims=True) + head_eps
    )
    ho_send[...] = (normed * hgain_ref[...] * head_scale).astype(bf16)
    for k in range(1, T):
        peer = lax.rem(t + k, T)
        send(
            None, ho_send.at[pl.ds(peer * rows, rows), :], ho.at[0, t], ho_ss.at[0], ho_rs.at[0], i, peer, False
        )
    for k in range(T):
        peer = lax.rem(t + k, T)
        send(
            None, ho_send.at[pl.ds(peer * rows, rows), :], ho.at[1, t], hx_ss.at[0], hx_rs.at[0], across, peer, False
        )
    ho[0, pl.ds(t, 1)] = ho_send[pl.ds(t * rows, rows), :][None]

    for d in range(3, Z):
        wo_stage(d)
    drain()
    sent_all(lat.at[pl.ds(0, over_rows), :], lat_yss.at[0])
    sent_all(part.at[pl.ds(0, S - 1)], part_ss.at[0])
    sent_all(terms.at[pl.ds(0, T - 1)], term_ss.at[0])
    for d in range(1, Z):
        wo_mate(d)
    twin_rows = (T - 1) * VALUE
    twin_view = wo.at[pl.ds(0, twin_rows), pl.ds(0, quarter_cols)]
    arrived(twin_view, wo_tss.at[0], wo_trs.at[0])
    pending[:] = late
    drain()
    sent_all(wo.at[pl.ds(0, Z * VALUE - weight_step), pl.ds(0, quarter_cols)], wo_yss.at[0])
    arrived(ho.at[0, pl.ds(0, T - 1)], ho_ss.at[0], ho_rs.at[0])
    arrived(ho.at[1], hx_ss.at[0], hx_rs.at[0])
    heads = jnp.concatenate(
        [jnp.concatenate([ho[which, h] for h in range(T)], axis=1) for which in (1, 0)], axis=0
    )
    near = []
    blocks = T // 2
    per_piece = blocks // FAR_PIECES
    for j in range(blocks):
        gated = terms[pl.ds(side * blocks + j, 1), 4:5, :][0] * jnp.dot(
            heads, wo[:, j * width : (j + 1) * width], preferred_element_type=f32
        )
        far_send[:, j * width : (j + 1) * width] = gated[:rows].astype(bf16)
        near.append(gated[rows:])
        if (j + 1) % per_piece == 0:
            n = j // per_piece
            piece = pl.ds(n * per_piece * width, per_piece * width)
            send(
                None, far_send.at[:, piece], far_recv.at[:, piece], far_ss.at[n], far_rs.at[n], across, t
            )
    for j in range(blocks):
        cols = pl.ds(pl.multiple_of(side * half + j * width, width), width)
        out_ref[:, cols] = (lat_ref[:, cols].astype(f32) + near[j]).astype(bf16)
    sent_all(twin_view, wo_tss.at[0])
    sent_all(ho.at[0, pl.ds(0, T - 1)], ho_ss.at[0])
    sent_all(ho.at[1], hx_ss.at[0])
    for n in range(FAR_PIECES):
        piece = pl.ds(n * per_piece * width, per_piece * width)
        arrived(far_recv.at[:, piece], far_ss.at[n], far_rs.at[n])
        for j in range(n * per_piece, (n + 1) * per_piece):
            cols = pl.ds(pl.multiple_of((1 - side) * half + j * width, width), width)
            out_ref[:, cols] = (
                lat_ref[:, cols].astype(f32)
                + far_recv[:, j * width : (j + 1) * width].astype(f32)
            ).astype(bf16)

    drain()


def fused_shards(S, T, *args):
    (latents, context, condition, context_condition, norm_gain, shift_weight, scale_weight,
     gate_weight, query_weight, key_weight, value_weight, subtract_share, head_gain,
     output_weight) = args
    rows, D = latents.shape
    crows = context.shape[0]
    count = rows * T
    bf16, f32 = jnp.bfloat16, jnp.float32
    vmem = pl.BlockSpec(memory_space=pltpu.VMEM)
    hbm = pl.BlockSpec(memory_space=pl.ANY)
    smem = pl.BlockSpec(memory_space=pltpu.SMEM)
    dma = pltpu.SemaphoreType.DMA
    return pl.pallas_call(
        functools.partial(fused_kernel, S=S, T=T),
        out_shape=jax.ShapeDtypeStruct((rows, D), bf16),
        in_specs=[vmem] * 5 + [hbm] * 6 + [smem, vmem, hbm],
        out_specs=vmem,
        scratch_shapes=[
            pltpu.VMEM((count, D), bf16),
            pltpu.VMEM((count, D), bf16),
            pltpu.VMEM((crows, D), bf16),
            pltpu.VMEM((D, 3 * VALUE), bf16),
            pltpu.VMEM((T * VALUE, D // 2), bf16),
            pltpu.VMEM((S, 8, D // T), f32),
            pltpu.VMEM((T, 8, D // T), f32),
            pltpu.VMEM((2, count, VALUE), f32),
            pltpu.VMEM((2 * count, VALUE), bf16),
            pltpu.VMEM((S, count + crows, 2 * VALUE), bf16),
            pltpu.VMEM((count, VALUE), bf16),
            pltpu.VMEM((2, T, rows, VALUE), bf16),
            pltpu.VMEM(shift_weight.shape, bf16),
            pltpu.VMEM(shift_weight.shape, bf16),
            pltpu.VMEM(shift_weight.shape, bf16),
            pltpu.VMEM((rows, D // 2), bf16),
            pltpu.VMEM((rows, D // 2), bf16),
            dma((7,)), dma((CHUNKS, T // 2 + 2)), dma((CHUNKS, T // 2 + 1)), dma((1,)), dma((1,)),
            dma((1,)), dma((1,)), dma((1,)), dma((1,)),
            dma((3,)), dma((S,)), dma((3,)), dma((S,)),
            dma((1,)), dma((1,)), dma((1,)), dma((1,)),
            dma((WEIGHT_CHUNKS, T // 2 + 2)), dma((WEIGHT_CHUNKS, T // 2)),
            dma((WEIGHT_CHUNKS, T // 2)), dma((1,)), dma((1,)), dma((1,)),
            dma((FAR_PIECES,)), dma((FAR_PIECES,)),
        ],
        compiler_params=pltpu.CompilerParams(
            collective_id=0, has_side_effects=True, vmem_limit_bytes=56 * 1024 * 1024
        ),
    )(latents, context, condition[None, :], context_condition[None, :], norm_gain[None, :],
      shift_weight, scale_weight, gate_weight, query_weight, key_weight, value_weight,
      subtract_share, head_gain[None, :], output_weight)


def fits(S, T, shapes):
    rows = shapes[0][0] // (S * T)
    crows = shapes[1][0] // S
    D = shapes[0][1]
    heads = shapes[8][1] // VALUE
    return (
        S == 4 and T % (2 * FAR_PIECES) == 0 and heads == T and rows % 16 == 0
        and crows % 16 == 0 and D % (128 * T) == 0 and D % (128 * CHUNKS) == 0 and T >= 8
        and rows * T * D * 8 + T * VALUE * D * 2 < 24 * 1024 * 1024
    )


def solution(mesh):
    in_specs = (
        P(("sp", "tp"), None),
        P("sp", None),
        P("sp"),
        P("sp"),
        P(),
        P("sp", "tp"),
        P("sp", "tp"),
        P("sp", "tp"),
        P(None, "tp"),
        P(None, "tp"),
        P(None, "tp"),
        P("tp"),
        P(),
        P("tp", None),
    )
    out_specs = P(("sp", "tp"), None)
    S, T = mesh.shape["sp"], mesh.shape["tp"]

    def whole(*args):
        if fits(S, T, [a.shape for a in args]):
            body = functools.partial(fused_shards, S, T)
        else:
            body = shards
        return jax.shard_map(
            body, mesh=mesh, in_specs=in_specs, out_specs=out_specs, check_vma=False
        )(*args)

    return whole
```

profile of v0, /device:TPU:0, one launch (start us, length us, event | category | flops | bytes accessed | tf_op | source)
XLA Modules:
  0.0 46.1 jit_solution(18019265372238286868)
XLA Ops:
  0.7 43.9 %shard_map.136 = bf16[32,2048]{1,0:T(8,128)(2,1)} custom-call(bf16[32,2048]{1,0:T(8,128)(2,1)} %lat_ref.1, bf16[64,2048]{1,0:T(8,128)(2,1)} %ctx_ref.1, f32[1,512]{1,0:T(1,128)} %bitcast.5, f32[1,512]{1,0:T(1,128)} %bitcast.6, f32[1,2048]{1,0:T(1,128)} %bitcast.4, bf16[512,256]{1,0:T(8,128)(2,1)} %shift_hbm.1, bf16[512,256]{1,0:T(8,128)(2,1)} %scale_hbm.1, ...), custom_call_target="tpu_custom_call" | custom-call | tf_op jit(solution)/shard_map/pallas_call | solution.py:545
  44.6 1.6 %copy.17 = bf16[32,2048]{1,0:T(8,128)(2,1)} copy(bf16[32,2048]{1,0:T(8,128)(2,1)} %shard_map.136) | data formatting | bytes 262144
where the time goes:
time: 46.3 us; the launch traced here: 46.1 us
  Pallas kernels  43.9 us (95%)
  local copies, waits for them, and re-layouts  1.57 us (3%)
  between operations  0.66 us (1%)
    pallas_call x1, Pallas kernels, fused_shards(): pl.pallas_call(functools.partial(fused_kernel, S=S, T=T), out_shape=jax.S...  43.9 us
    unnamed x1, local copies, waits for them, and re-layouts  1.57 us

commit v1 on v0

v1 whole, which is shorter than its diff:
```python
import functools
import math

import jax
import jax.numpy as jnp
from jax import lax
from jax.experimental import pallas as pl
from jax.experimental.pallas import tpu as pltpu
from jax.sharding import PartitionSpec as P

HEAD = 64
VALUE = 128
GRID_W = 64


norm_eps = 1e-06
head_eps = 1e-05
rope_theta = 10000.0
head_scale = 0.8


def rotary_tables(positions):
    quarter = HEAD // 4
    inverse = rope_theta ** (-2.0 * jnp.arange(quarter, dtype=jnp.float32) / (HEAD // 2))
    row_angle = (positions // GRID_W).astype(jnp.float32)[:, None] * inverse[None, :]
    column_angle = (positions % GRID_W).astype(jnp.float32)[:, None] * inverse[None, :]
    angles = jnp.concatenate([row_angle, row_angle, column_angle, column_angle], axis=-1)
    return (jnp.cos(angles), jnp.sin(angles))


def rotate(vectors, cosine, sine_table):
    quarter = HEAD // 4
    pieces = vectors.reshape(vectors.shape[:-1] + (2, 2, quarter))
    turned = jnp.concatenate([-pieces[..., 1:, :], pieces[..., :1, :]], axis=-2).reshape(
        vectors.shape
    )
    return vectors * cosine[:, None, :] + turned * sine_table[:, None, :]


def modulate(token_rows, gain_row, shift_row, scale_row):
    widened = token_rows.astype(jnp.float32)
    normed = widened * lax.rsqrt(jnp.mean(widened * widened, axis=-1, keepdims=True) + norm_eps)
    return (normed * gain_row * (1.0 + scale_row) + shift_row).astype(jnp.bfloat16)


def shards(
    latents,
    context,
    condition,
    context_condition,
    norm_gain,
    shift_weight,
    scale_weight,
    gate_weight,
    query_weight,
    key_weight,
    value_weight,
    subtract_share,
    head_gain,
    output_weight,
):
    activated = jax.nn.silu(jnp.stack([condition, context_condition])).astype(jnp.bfloat16)
    partial_terms = jnp.stack(
        [
            jnp.dot(activated, matrix, preferred_element_type=jnp.float32)
            for matrix in (shift_weight, scale_weight, gate_weight)
        ]
    )
    summed = lax.psum(partial_terms, "sp")
    full_terms = lax.all_gather(summed, "tp", axis=2, tiled=True)
    shift_terms, scale_terms, gate_terms = (full_terms[0], full_terms[1], full_terms[2])
    pair_weight = jnp.concatenate([key_weight, value_weight], axis=1)
    joined = jnp.concatenate([query_weight, pair_weight], axis=1)
    projected = jnp.dot(
        modulate(
            lax.all_gather(latents, "tp", axis=0, tiled=True),
            norm_gain,
            shift_terms[0],
            scale_terms[0],
        ),
        joined,
        preferred_element_type=jnp.float32,
    )
    local_count = projected.shape[0]
    positions = lax.axis_index("sp") * local_count + jnp.arange(local_count, dtype=jnp.int32)
    cosine, sine_table = rotary_tables(positions)
    queries = rotate(projected[:, :VALUE].reshape(local_count, 2, HEAD), cosine, sine_table)
    queries = queries.reshape(local_count, VALUE).astype(jnp.bfloat16)
    latent_keys = rotate(
        projected[:, VALUE : 2 * VALUE].reshape(local_count, 2, HEAD), cosine, sine_table
    )
    latent_keys = latent_keys.reshape(local_count, VALUE).astype(jnp.bfloat16)
    latent_pairs = jnp.concatenate(
        [latent_keys, projected[:, 2 * VALUE :].astype(jnp.bfloat16)], axis=1
    )
    context_mod = modulate(context, norm_gain, shift_terms[1], scale_terms[1])
    context_pairs = jnp.dot(context_mod, pair_weight, preferred_element_type=jnp.float32).astype(
        jnp.bfloat16
    )
    sent_pairs = jnp.concatenate([latent_pairs, context_pairs], axis=0)
    arrived = lax.all_gather(sent_pairs, "sp", axis=0, tiled=True)
    updated_carry = []
    for which_map in range(2):
        offset = which_map * HEAD
        scores = jnp.einsum(
            "qd,kd->qk",
            queries[:, offset : offset + HEAD],
            arrived[:, offset : offset + HEAD],
            preferred_element_type=jnp.float32,
        ) * HEAD ** (-0.5)
        powers = jnp.exp(scores)
        updated_carry.append(
            jnp.dot(
                powers.astype(jnp.bfloat16), arrived[:, VALUE:], preferred_element_type=jnp.float32
            )
        )
        updated_carry.append(jnp.sum(powers, axis=1, keepdims=True))
    first_sum, first_total, second_sum, second_total = tuple(updated_carry)
    share_value = subtract_share[0]
    difference = first_sum / first_total - share_value * (second_sum / second_total)
    normed = difference * lax.rsqrt(
        jnp.mean(difference * difference, axis=1, keepdims=True) + head_eps
    )
    head_output = (normed * head_gain * head_scale).astype(jnp.bfloat16)
    branch = lax.psum_scatter(
        jnp.dot(head_output, output_weight, preferred_element_type=jnp.float32),
        "tp",
        scatter_dimension=0,
        tiled=True,
    )
    return (latents.astype(jnp.float32) + gate_terms[0] * branch).astype(jnp.bfloat16)


MESH = pl.DeviceIdType.MESH
CHUNKS = 4
FAR_PIECES = 2
VMEM_LIMIT = 56 * 1024 * 1024


def fused_kernel(
    lat_hbm, ctx_hbm, cond_hbm, ccond_hbm, gain_hbm, shift_hbm, scale_hbm, gate_hbm,
    wq_hbm, wk_hbm, wv_hbm, share_hbm, hgain_hbm, wo_hbm, out_ref,
    ctx_ref, cond_ref, ccond_ref, gain_ref, share_ref, hgain_ref, lat, mod, cmod, wqkv, wo, wo_own,
    part, terms, tables, queries, kv, ho_send, ho, shift_ref, scale_ref, gate_ref, far_send, far_recv,
    load_sem, lat_ss, lat_rs, lat_xrs, lat_yss, lat_yrs, part_ss, part_rs, term_ss, term_rs, chain_sem,
    kv_ss, kv_rs, ckv_ss, ckv_rs, ho_ss, ho_rs, wo_mss, wo_ss, wo_rs, wo_xss, wo_xrs, wo_tss, wo_trs,
    far_ss, far_rs,
    *, S, T,
):
    f32, bf16 = jnp.float32, jnp.bfloat16
    count, D = lat.shape
    rows = count // T
    crows = ctx_ref.shape[0]
    width = D // T
    half = D // 2
    strip = half // S
    Z = T // 2
    i = lax.axis_index("sp")
    t = lax.axis_index("tp")
    z = lax.div(t, 2)
    y = lax.rem(t, 2)
    mate = t + 1 - 2 * y
    twin = i + 1 - 2 * lax.rem(i, 2)
    across = lax.rem(i + 2, S)
    twin_across = lax.rem(twin + 2, S)
    inner = jnp.logical_and(z > 0, z < Z - 1)
    outer = jnp.logical_or(z == 0, z == Z - 1)
    pending = []

    def when(cond, action):
        if cond is None:
            action()
        else:
            pl.when(cond)(action)

    def copy(src, dst, ss, rs, sp, tp):
        return pltpu.make_async_remote_copy(
            src_ref=src, dst_ref=dst, send_sem=ss, recv_sem=rs,
            device_id={"sp": sp, "tp": tp}, device_id_type=MESH,
        )

    def send(cond, src, dst, ss, rs, sp, tp, tracked=True):
        made = copy(src, dst, ss, rs, sp, tp)

        def go():
            made.start()

        when(cond, go)
        if tracked:
            pending.append((cond, made))

    def drain():
        for cond, made in pending:
            def finish(made=made):
                made.wait_send()

            when(cond, finish)
        pending.clear()

    def sent_all(view, ss):
        copy(view, view, ss, ss, twin, t).wait_send()

    def arrived(dst, ss, rs):
        copy(dst, dst, ss, rs, twin, t).wait_recv()

    def load(k, src, dst):
        return pltpu.make_async_copy(src, dst, load_sem.at[k])

    def half_cols(which):
        return pl.ds(pl.multiple_of(which * half, half), half)

    def strip_cols(which, share):
        return pl.ds(pl.multiple_of(which * half + share * strip, strip), strip)

    own_rows = pl.ds(pl.multiple_of(t * rows, rows), rows)
    own_load = load(0, lat_hbm, lat.at[own_rows, :])
    cond_loads = [load(1, cond_hbm, cond_ref), load(2, ccond_hbm, ccond_ref)]
    term_loads = [
        load(3, shift_hbm, shift_ref), load(4, scale_hbm, scale_ref), load(5, gate_hbm, gate_ref)
    ]
    qkv_loads = [
        load(6, wq_hbm, wqkv.at[:, pl.ds(0, VALUE)]),
        load(7, wk_hbm, wqkv.at[:, pl.ds(VALUE, VALUE)]),
        load(8, wv_hbm, wqkv.at[:, pl.ds(2 * VALUE, VALUE)]),
        load(9, ctx_hbm, ctx_ref),
        load(10, gain_hbm, gain_ref),
        load(11, share_hbm, share_ref),
        load(12, hgain_hbm, hgain_ref),
    ]
    wo_strip = load(13, wo_hbm.at[:, strip_cols(1 - y, i)], wo_own)
    wo_half = load(15, wo_hbm.at[:, half_cols(y)], wo.at[pl.ds(t * VALUE, VALUE), :])

    barrier = pltpu.get_barrier_semaphore()

    def greet(cond, sp, tp):
        def go():
            pl.semaphore_signal(
                barrier, inc=1, device_id={"sp": sp, "tp": tp}, device_id_type=MESH
            )

        when(cond, go)

    greet(z > 0, i, t - 2)
    greet(z < Z - 1, i, t + 2)
    greet(None, i, mate)
    for peer in (across, twin_across, twin):
        greet(None, peer, t)
    for made in [own_load] + cond_loads + term_loads + [wo_strip, wo_half] + qkv_loads:
        made.start()
    pl.semaphore_wait(
        barrier, 4 + (z > 0).astype(jnp.int32) + (z < Z - 1).astype(jnp.int32)
    )
    def chain(cond, which, tp):
        def go():
            pl.semaphore_signal(
                chain_sem.at[which], inc=1, device_id={"sp": i, "tp": tp}, device_id_type=MESH
            )

        when(cond, go)

    def chained(cond, which):
        def go():
            pl.semaphore_wait(chain_sem.at[which], 1)

        when(cond, go)

    below = z < Z - 1 - z
    inward = jnp.where(below, t + 4, t - 4)
    midward = jnp.where(below, t + 2, t - 2)
    outward = jnp.where(below, t - 2, t + 2)
    chain(inner, 0, outward)
    chain(outer, 1, midward)
    own_load.wait()

    step = D // CHUNKS

    def lat_piece(block, c):
        return lat.at[pl.ds(pl.multiple_of(block * rows, rows), rows), pl.ds(c * step, step)]

    def wo_piece(head, share):
        return wo.at[
            pl.ds(pl.multiple_of(head * VALUE, VALUE), VALUE),
            pl.ds(pl.multiple_of(share * strip, strip), strip),
        ]

    upper = range(CHUNKS // 2, CHUNKS)
    for c in range(CHUNKS):
        own = lat_piece(t, c)
        send(z < Z - 1, own, own, lat_ss.at[c, 0], lat_rs.at[c, z], i, t + 2)
        send(z > 0, own, own, lat_ss.at[c, 1], lat_rs.at[c, z], i, t - 2)
        rs = lat_rs.at[c, Z] if c in upper else lat_yrs.at[0]
        send(None, own, own, lat_yss.at[0], rs, i, mate, False)

    wo_strip.wait()
    send(None, wo_own, wo_piece(t, i), wo_mss.at[0], wo_rs.at[t], i, mate, False)

    def lat_far():
        for c in range(CHUNKS):
            own = lat_piece(t, c)
            send(outer, own, own, lat_ss.at[c, 2], lat_rs.at[c, z], i, inward)

    def lat_cross():
        for c in upper:
            piece = lat_piece(mate, c)
            arrived(piece, lat_yss.at[0], lat_rs.at[c, Z])
            send(outer, piece, piece, lat_ss.at[c, 3], lat_xrs.at[c], i, inward)

    def lat_stage(d, chunks=range(CHUNKS)):
        for c in chunks:
            for sign in (-1, 1):
                block = t + 2 * d * sign
                here = z - d >= 0 if sign < 0 else z + d < Z
                piece = lat_piece(block, c)
                layer = z + d * sign
                rs = lat_rs.at[c, layer]

                def come(piece=piece, rs=rs):
                    arrived(piece, lat_yss.at[0], rs)

                when(here, come)
                if d < Z - 1:
                    onward = jnp.logical_and(here, jnp.logical_and(inner, below == (sign > 0)))
                    send(onward, piece, piece, lat_ss.at[c, 1 + d], rs, i, outward)
                over = here
                if d > 1 and c in upper:
                    over = jnp.logical_and(here, outer)
                if d < Z - 1 or c not in upper:
                    send(over, piece, piece, lat_yss.at[0], lat_yrs.at[0], i, mate, False)

    def lat_last():
        opposite = 2 * (Z - 1 - z) + 1 - y
        for c in upper:
            for where, block in ((outer, opposite), (inner, mate + inward - t)):
                piece = lat_piece(block, c)

                def come(piece=piece, c=c):
                    arrived(piece, lat_yss.at[0], lat_xrs.at[c])

                when(where, come)
                if where is inner:
                    send(inner, piece, piece, lat_ss.at[c, 4], lat_xrs.at[c], i, outward)

    def wo_launch(cond, head, tp):
        piece = wo_piece(head, i)
        send(cond, piece, piece, wo_ss.at[0], wo_rs.at[head], i, tp, False)

    def wo_heads(d, sign):
        layer = 2 * (z + d * sign)
        return (layer + y, layer + 1 - y)

    def wo_take(cond, head, spread=True, onward=None):
        def go():
            piece = wo_piece(head, i)
            arrived(piece, wo_ss.at[0], wo_rs.at[head])

        def share():
            piece = wo_piece(head, i)
            copy(piece, piece, wo_xss.at[0], wo_xrs.at[head], across, t).start()
            copy(piece, piece, wo_tss.at[0], wo_trs.at[0], twin, t).start()

        when(cond, go)
        if onward is not None:
            wo_launch(onward, head, outward)
        if spread:
            when(cond, share)

    def wo_stage(d, where, middle=None):
        for sign in (-1, 1):
            here = z - d >= 0 if sign < 0 else z + d < Z
            here = jnp.logical_and(here, where)
            if middle is not None:
                here = jnp.logical_and(here, (below == (sign > 0)) == middle)
            onward = None
            if d < Z - 1:
                onward = jnp.logical_and(here, jnp.logical_and(inner, below == (sign > 0)))
            for head in wo_heads(d, sign):
                wo_take(here, head, True, onward)

    def wo_relay(d, where=None):
        todo = [(None, mate)] if d == 0 else [
            (z - d >= 0 if sign < 0 else z + d < Z, head)
            for sign in (-1, 1) for head in wo_heads(d, sign)
        ]
        for cond, head in todo:
            def go(head=head):
                piece = wo_piece(head, across)
                arrived(piece, wo_ss.at[0], wo_xrs.at[head])
                copy(piece, piece, wo_tss.at[0], wo_trs.at[0], twin, t).start()

            when(cond, go)

    def silu(v):
        return v / (1.0 + jnp.exp(-v))

    for made in cond_loads:
        made.wait()
    depth = cond_ref.shape[1]
    line = lax.broadcasted_iota(jnp.int32, (8, depth), 0)
    act0 = jnp.broadcast_to(silu(cond_ref[...]), (8, depth))
    act1 = jnp.broadcast_to(silu(ccond_ref[...]), (8, depth))

    def two_lines(first, matrix_ref, with_second):
        left = jnp.where(line == first, act0, 0.0)
        if with_second:
            left = jnp.where(line == first + 1, act1, left)
        return jnp.dot(left.astype(bf16), matrix_ref[...], preferred_element_type=f32)

    for made in term_loads:
        made.wait()
    part[pl.ds(i, 1)] = (
        two_lines(0, shift_ref, True) + two_lines(2, scale_ref, True) + two_lines(4, gate_ref, False)
    )[None]
    for k in range(1, S):
        send(None, part.at[i], part.at[i], part_ss.at[0], part_rs.at[0], lax.rem(i + k, S), t, False)

    lane = lax.broadcasted_iota(jnp.int32, (count, VALUE), 1)
    place = i * count + lax.broadcasted_iota(jnp.int32, (count, VALUE), 0)
    spot = lax.rem(lane, HEAD)
    quarter = HEAD // 4
    power = lax.rem(spot, quarter).astype(f32) * (-2.0 / (HEAD // 2))
    inverse = jnp.exp(power * math.log(rope_theta))
    along = jnp.where(spot < HEAD // 2, lax.div(place, GRID_W), lax.rem(place, GRID_W))
    angle = along.astype(f32) * inverse
    even = lax.rem(lax.div(spot, quarter), 2) == 0
    tables[0] = jnp.cos(angle)
    tables[1] = jnp.sin(angle)

    chained(outer, 0)
    lat_far()
    chained(inner, 1)
    chain(inner, 2, midward)
    chained(inner, 2)
    chain(inner, 2, outward)
    lat_stage(1, range(CHUNKS // 2))
    chained(outer, 2)

    arrived(part.at[pl.ds(0, S - 1)], part_ss.at[0], part_rs.at[0])
    total = part[0]
    for k in range(1, S):
        total = total + part[k]
    terms[pl.ds(t, 1)] = total[None]
    for k in range(1, T):
        send(
            None, terms.at[t], terms.at[t], term_ss.at[0], term_rs.at[0], i, lax.rem(t + k, T), False
        )

    lat_stage(1, range(CHUNKS // 2, CHUNKS))
    lat_cross()
    wo_half.wait()
    wo_take(None, mate)
    for head in (t, mate):
        wo_launch(None, head, midward)
    for d in range(2, Z):
        lat_stage(d)
        if d == 2:
            for head in (t, mate):
                wo_launch(outer, head, inward)
            wo_launch(inner, t, outward)
    lat_last()
    wo_launch(inner, mate, outward)
    wo_stage(1, inner, True)

    def modulate_into(dst, src, first, n, which):
        wide = src[...].astype(f32)
        factor = lax.rsqrt(jnp.mean(wide * wide, axis=-1, keepdims=True) + norm_eps)
        for j in range(T):
            cols = slice(j * width, (j + 1) * width)
            mult = gain_ref[:, cols] * (1.0 + terms[j, 2 + which : 3 + which, :])
            shifted = wide[:, cols] * factor * mult + terms[j, which : which + 1, :]
            dst[pl.ds(first, n), cols] = shifted.astype(bf16)

    for made in qkv_loads:
        made.wait()
    arrived(terms.at[pl.ds(0, T - 1)], term_ss.at[0], term_rs.at[0])
    modulate_into(cmod, ctx_ref, 0, crows, 1)
    kv[pl.ds(i, 1), pl.ds(count, crows), :] = jnp.dot(
        cmod[...], wqkv[:, VALUE:], preferred_element_type=f32
    ).astype(bf16)[None]

    def ckv_piece(s):
        return kv.at[s, pl.ds(count, crows), :]

    def kv_piece(s):
        return kv.at[s, pl.ds(0, count), :]

    send(None, ckv_piece(i), ckv_piece(i), ckv_ss.at[0], ckv_rs.at[i], across, t)
    send(None, ckv_piece(i), ckv_piece(i), ckv_ss.at[1], ckv_rs.at[i], twin, t)

    def over_view(where, less):
        return lat.at[pl.ds(0, Z * rows - rows + less), :]

    for where in (outer, inner):
        def come(where=where):
            arrived(over_view(where, 0), lat_yss.at[0], lat_yrs.at[0])

        when(where, come)
    modulate_into(mod, lat, 0, count, 0)
    projected = jnp.dot(mod[...], wqkv[...], preferred_element_type=f32)

    def rotated(u):
        turned = jnp.where(even, -pltpu.roll(u, VALUE - quarter, 1), pltpu.roll(u, quarter, 1))
        return u * tables[0] + turned * tables[1]

    kv[pl.ds(i, 1), pl.ds(0, count), pl.ds(0, VALUE)] = (
        rotated(projected[:, VALUE : 2 * VALUE]).astype(bf16)[None]
    )
    kv[pl.ds(i, 1), pl.ds(0, count), pl.ds(VALUE, VALUE)] = (
        projected[:, 2 * VALUE :].astype(bf16)[None]
    )
    send(None, kv_piece(i), kv_piece(i), kv_ss.at[0], kv_rs.at[i], across, t)
    send(None, kv_piece(i), kv_piece(i), kv_ss.at[1], kv_rs.at[i], twin, t)
    query = rotated(projected[:, :VALUE]).astype(bf16) * jnp.asarray(HEAD ** (-0.5), bf16)
    first_half = lane < HEAD
    zero = jnp.zeros_like(query)
    queries[0:count, :] = jnp.where(first_half, query, zero)
    queries[count:, :] = jnp.where(first_half, zero, query)

    ones = jnp.ones((count + crows, VALUE), bf16)

    def attend(slot):
        rows_kv = kv[slot]
        scores = lax.dot_general(
            queries[...], rows_kv[:, :VALUE], (((1,), (1,)), ((), ())), preferred_element_type=f32
        )
        return jnp.dot(
            jnp.exp(scores).astype(bf16),
            jnp.concatenate([rows_kv[:, VALUE:], ones], axis=1),
            preferred_element_type=f32,
        )

    sums = attend(i)
    arrived(ckv_piece(across), ckv_ss.at[2], ckv_rs.at[across])
    send(None, ckv_piece(across), ckv_piece(across), ckv_ss.at[2], ckv_rs.at[across], twin, t)
    wo_stage(2, inner)
    wo_relay(0)
    wo_stage(1, outer)
    arrived(kv_piece(twin), kv_ss.at[2], kv_rs.at[twin])
    arrived(ckv_piece(twin), ckv_ss.at[2], ckv_rs.at[twin])
    sums = sums + attend(twin)
    arrived(kv_piece(across), kv_ss.at[2], kv_rs.at[across])
    send(None, kv_piece(across), kv_piece(across), kv_ss.at[2], kv_rs.at[across], twin, t)
    wo_stage(1, inner, False)
    wo_stage(2, outer)
    sums = sums + attend(across)
    arrived(kv_piece(twin_across), kv_ss.at[2], kv_rs.at[twin_across])
    arrived(ckv_piece(twin_across), ckv_ss.at[2], ckv_rs.at[twin_across])
    sums = sums + attend(twin_across)
    ratio = sums[:, :VALUE] / sums[:, VALUE:]
    difference = ratio[:count] - share_ref[...] * ratio[count:]
    normed = difference * lax.rsqrt(
        jnp.mean(difference * difference, axis=1, keepdims=True) + head_eps
    )
    ho_send[...] = (normed * hgain_ref[...] * head_scale).astype(bf16)

    def pair_rows(layer):
        return ho_send.at[pl.ds(pl.multiple_of(layer * 2 * rows, 2 * rows), 2 * rows), :]

    for k in range(1, T):
        peer = lax.rem(t + k, T)
        send(None, pair_rows(lax.div(peer, 2)), ho.at[t], ho_ss.at[0], ho_rs.at[0], i, peer, False)
    ho[pl.ds(t, 1)] = pair_rows(z)[...][None]

    wo_stage(3, outer)
    wo_relay(1)
    wo_relay(2)
    wo_relay(3)
    drain()
    for where in (outer, inner):
        def left(where=where):
            sent_all(over_view(where, rows // 2), lat_yss.at[0])

        when(where, left)
    sent_all(part.at[pl.ds(0, S - 1)], part_ss.at[0])
    sent_all(terms.at[pl.ds(0, T - 1)], term_ss.at[0])
    other_rows = pl.ds(0, (T - 1) * VALUE)
    sent_all(wo_own, wo_mss.at[0])

    def wo_sent(heads):
        def go():
            sent_all(wo.at[pl.ds(0, heads * VALUE), pl.ds(0, strip)], wo_ss.at[0])

        return go

    when(outer, wo_sent(4))
    when(inner, wo_sent(8))
    arrived(wo.at[other_rows, pl.ds(0, 2 * strip)], wo_tss.at[0], wo_trs.at[0])
    arrived(ho.at[pl.ds(0, T - 1)], ho_ss.at[0], ho_rs.at[0])
    heads = jnp.concatenate(
        [
            jnp.concatenate(
                [ho[h, pl.ds(pl.multiple_of(which * rows, rows), rows), :] for h in range(T)], axis=1
            )
            for which in (1 - y, y)
        ],
        axis=0,
    )
    near = []
    blocks = T // 2
    per_piece = blocks // FAR_PIECES
    for j in range(blocks):
        gated = terms[pl.ds(y * blocks + j, 1), 4:5, :][0] * jnp.dot(
            heads, wo[:, j * width : (j + 1) * width], preferred_element_type=f32
        )
        far_send[:, j * width : (j + 1) * width] = gated[:rows].astype(bf16)
        near.append(gated[rows:])
        if (j + 1) % per_piece == 0:
            n = j // per_piece
            piece = pl.ds(n * per_piece * width, per_piece * width)
            send(
                None, far_send.at[:, piece], far_recv.at[:, piece], far_ss.at[n], far_rs.at[n], i, mate
            )
    for j in range(blocks):
        cols = pl.ds(pl.multiple_of(y * half + j * width, width), width)
        out_ref[:, cols] = (lat[own_rows, cols].astype(f32) + near[j]).astype(bf16)
    sent_all(wo.at[other_rows, pl.ds(0, strip)], wo_xss.at[0])
    sent_all(wo.at[other_rows, pl.ds(0, 2 * strip)], wo_tss.at[0])
    sent_all(ho.at[pl.ds(0, T - 1)], ho_ss.at[0])
    for n in range(FAR_PIECES):
        piece = pl.ds(n * per_piece * width, per_piece * width)
        arrived(far_recv.at[:, piece], far_ss.at[n], far_rs.at[n])
        for j in range(n * per_piece, (n + 1) * per_piece):
            cols = pl.ds(pl.multiple_of((1 - y) * half + j * width, width), width)
            out_ref[:, cols] = (
                lat[own_rows, cols].astype(f32)
                + far_recv[:, j * width : (j + 1) * width].astype(f32)
            ).astype(bf16)

    drain()


def fused_shards(S, T, *args):
    (latents, context, condition, context_condition, norm_gain, shift_weight, scale_weight,
     gate_weight, query_weight, key_weight, value_weight, subtract_share, head_gain,
     output_weight) = args
    rows, D = latents.shape
    crows = context.shape[0]
    count = rows * T
    Z = T // 2
    bf16, f32 = jnp.bfloat16, jnp.float32
    vmem = pl.BlockSpec(memory_space=pltpu.VMEM)
    hbm = pl.BlockSpec(memory_space=pltpu.HBM)
    dma = pltpu.SemaphoreType.DMA
    return pl.pallas_call(
        functools.partial(fused_kernel, S=S, T=T),
        out_shape=jax.ShapeDtypeStruct((rows, D), bf16),
        in_specs=[hbm] * 14,
        out_specs=vmem,
        scratch_shapes=[
            pltpu.VMEM((crows, D), bf16),
            pltpu.VMEM((1, condition.shape[0]), f32),
            pltpu.VMEM((1, condition.shape[0]), f32),
            pltpu.VMEM((1, D), f32),
            pltpu.VMEM((1, 1), f32),
            pltpu.VMEM((1, VALUE), f32),
            pltpu.VMEM((count, D), bf16),
            pltpu.VMEM((count, D), bf16),
            pltpu.VMEM((crows, D), bf16),
            pltpu.VMEM((D, 3 * VALUE), bf16),
            pltpu.VMEM((T * VALUE, D // 2), bf16),
            pltpu.VMEM((VALUE, D // (2 * S)), bf16),
            pltpu.VMEM((S, 8, D // T), f32),
            pltpu.VMEM((T, 8, D // T), f32),
            pltpu.VMEM((2, count, VALUE), f32),
            pltpu.VMEM((2 * count, VALUE), bf16),
            pltpu.VMEM((S, count + crows, 2 * VALUE), bf16),
            pltpu.VMEM((count, VALUE), bf16),
            pltpu.VMEM((T, 2 * rows, VALUE), bf16),
            pltpu.VMEM(shift_weight.shape, bf16),
            pltpu.VMEM(shift_weight.shape, bf16),
            pltpu.VMEM(shift_weight.shape, bf16),
            pltpu.VMEM((rows, D // 2), bf16),
            pltpu.VMEM((rows, D // 2), bf16),
            dma((16,)), dma((CHUNKS, 5)), dma((CHUNKS, Z + 1)), dma((CHUNKS,)), dma((1,)), dma((1,)),
            dma((1,)), dma((1,)), dma((1,)), dma((1,)), pltpu.SemaphoreType.REGULAR((3,)),
            dma((3,)), dma((S,)), dma((3,)), dma((S,)),
            dma((1,)), dma((1,)), dma((1,)), dma((1,)), dma((T,)), dma((1,)), dma((T,)), dma((1,)), dma((1,)),
            dma((FAR_PIECES,)), dma((FAR_PIECES,)),
        ],
        compiler_params=pltpu.CompilerParams(
            collective_id=0, has_side_effects=True, vmem_limit_bytes=VMEM_LIMIT
        ),
    )(latents, context, condition[None, :], context_condition[None, :], norm_gain[None, :],
      shift_weight, scale_weight, gate_weight, query_weight, key_weight, value_weight,
      subtract_share[None, :], head_gain[None, :], output_weight)


def fits(S, T, shapes):
    rows = shapes[0][0] // (S * T)
    crows = shapes[1][0] // S
    D = shapes[0][1]
    heads = shapes[8][1] // VALUE
    return (
        S == 4 and T == 8 and heads == T and rows % 32 == 0
        and crows % 16 == 0 and D % (128 * T) == 0 and D % (128 * CHUNKS) == 0
        and rows * T * D * 8 + T * VALUE * D * 2 < 24 * 1024 * 1024
    )


def solution(mesh):
    in_specs = (
        P(("sp", "tp"), None),
        P("sp", None),
        P("sp"),
        P("sp"),
        P(),
        P("sp", "tp"),
        P("sp", "tp"),
        P("sp", "tp"),
        P(None, "tp"),
        P(None, "tp"),
        P(None, "tp"),
        P("tp"),
        P(),
        P("tp", None),
    )
    out_specs = P(("sp", "tp"), None)
    S, T = mesh.shape["sp"], mesh.shape["tp"]

    def whole(*args):
        if fits(S, T, [a.shape for a in args]):
            body = functools.partial(fused_shards, S, T)
        else:
            body = shards
        return jax.shard_map(
            body, mesh=mesh, in_specs=in_specs, out_specs=out_specs, check_vma=False
        )(*args)

    return whole
```

time: 46.3 us -> 42.7 us (0.922)
  Pallas kernels: 43.9 us -> 40.3 us
    pallas_call x1, Pallas kernels: 43.9 us -> 40.3 us  [fused_shards(): pl.pallas_call(functools.partial(fused_kernel, S=S, T=T), out_shape=jax.S...]
where the time goes in v1:
time: 42.7 us; the launch traced here: 42.5 us
  Pallas kernels  40.3 us (94%)
  local copies, waits for them, and re-layouts  1.57 us (4%)
  between operations  0.66 us (2%)
    pallas_call x1, Pallas kernels, fused_shards(): pl.pallas_call(functools.partial(fused_kernel, S=S, T=T), out_shape=jax.S...  40.3 us
    unnamed x1, local copies, waits for them, and re-layouts  1.57 us

profile of v1, /device:TPU:0, one launch (start us, length us, event | category | flops | bytes accessed | tf_op | source)
XLA Modules:
  0.0 42.5 jit_solution(15117477155095335807)
XLA Ops:
  0.7 40.3 %shard_map.136 = bf16[32,2048]{1,0:T(8,128)(2,1)} custom-call(bf16[32,2048]{1,0:T(8,128)(2,1)} %lat_hbm.1, bf16[64,2048]{1,0:T(8,128)(2,1)} %ctx_hbm.1, f32[1,512]{1,0:T(1,128)} %bitcast.7, f32[1,512]{1,0:T(1,128)} %bitcast.8, f32[1,2048]{1,0:T(1,128)} %bitcast.6, bf16[512,256]{1,0:T(8,128)(2,1)} %shift_hbm.1, bf16[512,256]{1,0:T(8,128)(2,1)} %scale_hbm.1, ...), custom_call_target="tpu_custom_call" | custom-call | tf_op jit(solution)/shard_map/pallas_call | solution.py:643
  40.9 1.6 %copy.17 = bf16[32,2048]{1,0:T(8,128)(2,1)} copy(bf16[32,2048]{1,0:T(8,128)(2,1)} %shard_map.136) | data formatting | bytes 262144

commit v2 on v1

--- a/solution.py
+++ b/solution.py
@@ -133,15 +133,15 @@
 
 MESH = pl.DeviceIdType.MESH
 CHUNKS = 4
-FAR_PIECES = 2
-VMEM_LIMIT = 56 * 1024 * 1024
+FAR_PIECES = 4
+VMEM_LIMIT = 55000 * 1024
 
 
 def fused_kernel(
     lat_hbm, ctx_hbm, cond_hbm, ccond_hbm, gain_hbm, shift_hbm, scale_hbm, gate_hbm,
     wq_hbm, wk_hbm, wv_hbm, share_hbm, hgain_hbm, wo_hbm, out_ref,
     ctx_ref, cond_ref, ccond_ref, gain_ref, share_ref, hgain_ref, lat, mod, cmod, wqkv, wo, wo_own,
-    part, terms, tables, queries, kv, ho_send, ho, shift_ref, scale_ref, gate_ref, far_send, far_recv,
+    part, terms, tables, queries, kv, ho_send, ho, shift_ref, scale_ref, gate_ref, far_send, far_recv, acc,
     load_sem, lat_ss, lat_rs, lat_xrs, lat_yss, lat_yrs, part_ss, part_rs, term_ss, term_rs, chain_sem,
     kv_ss, kv_rs, ckv_ss, ckv_rs, ho_ss, ho_rs, wo_mss, wo_ss, wo_rs, wo_xss, wo_xrs, wo_tss, wo_trs,
     far_ss, far_rs,
@@ -299,11 +299,13 @@
             own = lat_piece(t, c)
             send(outer, own, own, lat_ss.at[c, 2], lat_rs.at[c, z], i, inward)
 
+    opposite = 2 * (Z - 1 - z) + y
+
     def lat_cross():
         for c in upper:
             piece = lat_piece(mate, c)
             arrived(piece, lat_yss.at[0], lat_rs.at[c, Z])
-            send(outer, piece, piece, lat_ss.at[c, 3], lat_xrs.at[c], i, inward)
+            send(outer, piece, piece, lat_ss.at[c, 3], lat_xrs.at[c], i, opposite)
 
     def lat_stage(d, chunks=range(CHUNKS)):
         for c in chunks:
@@ -321,24 +323,16 @@
                 if d < Z - 1:
                     onward = jnp.logical_and(here, jnp.logical_and(inner, below == (sign > 0)))
                     send(onward, piece, piece, lat_ss.at[c, 1 + d], rs, i, outward)
-                over = here
-                if d > 1 and c in upper:
-                    over = jnp.logical_and(here, outer)
                 if d < Z - 1 or c not in upper:
-                    send(over, piece, piece, lat_yss.at[0], lat_yrs.at[0], i, mate, False)
+                    batch = jnp.where((2 * layer < Z) == below, 0, 1)
+                    send(here, piece, piece, lat_yss.at[0], lat_yrs.at[batch], i, mate, False)
 
     def lat_last():
-        opposite = 2 * (Z - 1 - z) + 1 - y
-        for c in upper:
-            for where, block in ((outer, opposite), (inner, mate + inward - t)):
-                piece = lat_piece(block, c)
-
-                def come(piece=piece, c=c):
-                    arrived(piece, lat_yss.at[0], lat_xrs.at[c])
-
-                when(where, come)
-                if where is inner:
-                    send(inner, piece, piece, lat_ss.at[c, 4], lat_xrs.at[c], i, outward)
+        def come():
+            for c in upper:
+                arrived(lat_piece(opposite + mate - t, c), lat_yss.at[0], lat_xrs.at[c])
+
+        when(outer, come)
 
     def wo_launch(cond, head, tp):
         piece = wo_piece(head, i)
@@ -348,23 +342,28 @@
         layer = 2 * (z + d * sign)
         return (layer + y, layer + 1 - y)
 
-    def wo_take(cond, head, spread=True, onward=None):
+    def late_head(head):
+        layer = lax.div(head, 2)
+        return jnp.where(layer == jnp.where(below, Z - 1, 0), 1, 0)
+
+    def wo_take(cond, head, onward=None):
         def go():
             piece = wo_piece(head, i)
             arrived(piece, wo_ss.at[0], wo_rs.at[head])
 
-        def share():
-            piece = wo_piece(head, i)
-            copy(piece, piece, wo_xss.at[0], wo_xrs.at[head], across, t).start()
-            copy(piece, piece, wo_tss.at[0], wo_trs.at[0], twin, t).start()
-
         when(cond, go)
         if onward is not None:
             wo_launch(onward, head, outward)
-        if spread:
-            when(cond, share)
-
-    def wo_stage(d, where, middle=None):
+
+    def wo_share(cond, head):
+        def go():
+            piece = wo_piece(head, i)
+            copy(piece, piece, wo_xss.at[0], wo_xrs.at[head], across, t).start()
+            copy(piece, piece, wo_tss.at[0], wo_trs.at[late_head(head)], twin, t).start()
+
+        when(cond, go)
+
+    def wo_stage(d, where, middle=None, take=True, share=True):
         for sign in (-1, 1):
             here = z - d >= 0 if sign < 0 else z + d < Z
             here = jnp.logical_and(here, where)
@@ -374,7 +373,10 @@
             if d < Z - 1:
                 onward = jnp.logical_and(here, jnp.logical_and(inner, below == (sign > 0)))
             for head in wo_heads(d, sign):
-                wo_take(here, head, True, onward)
+                if take:
+                    wo_take(here, head, onward)
+                if share:
+                    wo_share(here, head)
 
     def wo_relay(d, where=None):
         todo = [(None, mate)] if d == 0 else [
@@ -385,7 +387,7 @@
             def go(head=head):
                 piece = wo_piece(head, across)
                 arrived(piece, wo_ss.at[0], wo_xrs.at[head])
-                copy(piece, piece, wo_tss.at[0], wo_trs.at[0], twin, t).start()
+                copy(piece, piece, wo_tss.at[0], wo_trs.at[late_head(head)], twin, t).start()
 
             when(cond, go)
 
@@ -448,17 +450,14 @@
     lat_cross()
     wo_half.wait()
     wo_take(None, mate)
+    wo_share(None, mate)
     for head in (t, mate):
         wo_launch(None, head, midward)
-    for d in range(2, Z):
-        lat_stage(d)
-        if d == 2:
-            for head in (t, mate):
-                wo_launch(outer, head, inward)
-            wo_launch(inner, t, outward)
-    lat_last()
+        wo_launch(outer, head, inward)
+    lat_stage(2)
+    wo_launch(inner, t, outward)
     wo_launch(inner, mate, outward)
-    wo_stage(1, inner, True)
+    lat_stage(3, range(CHUNKS // 2))
 
     def modulate_into(dst, src, first, n, which):
         wide = src[...].astype(f32)
@@ -469,6 +468,50 @@
             shifted = wide[:, cols] * factor * mult + terms[j, which : which + 1, :]
             dst[pl.ds(first, n), cols] = shifted.astype(bf16)
 
+    def ckv_piece(s):
+        return kv.at[s, pl.ds(count, crows), :]
+
+    part_rows = count // 2
+    batch_first = [
+        pl.multiple_of(jnp.where(below == (b == 0), 0, part_rows), part_rows) for b in range(2)
+    ]
+
+    def kv_piece(s, b):
+        return kv.at[s, pl.ds(batch_first[b], part_rows), :]
+
+    first_half = lax.broadcasted_iota(jnp.int32, (part_rows, VALUE), 1) < HEAD
+
+    def project_batch(b):
+        first = batch_first[b]
+        which = pl.ds(first, part_rows)
+        modulate_into(mod, lat.at[which, :], 0, part_rows, 0)
+        projected = jnp.dot(mod[...], wqkv[...], preferred_element_type=f32)
+
+        def rotated(u):
+            turned = jnp.where(
+                even[:part_rows], -pltpu.roll(u, VALUE - quarter, 1), pltpu.roll(u, quarter, 1)
+            )
+            return u * tables[0, which, :] + turned * tables[1, which, :]
+
+        kv[pl.ds(i, 1), which, pl.ds(0, VALUE)] = (
+            rotated(projected[:, VALUE : 2 * VALUE]).astype(bf16)[None]
+        )
+        kv[pl.ds(i, 1), which, pl.ds(VALUE, VALUE)] = projected[:, 2 * VALUE :].astype(bf16)[None]
+        own = kv_piece(i, b)
+        send(None, own, own, kv_ss.at[b, 0], kv_rs.at[b, i], across, t)
+        send(None, own, own, kv_ss.at[b, 1], kv_rs.at[b, i], twin, t)
+        query = rotated(projected[:, :VALUE]).astype(bf16) * jnp.asarray(HEAD ** (-0.5), bf16)
+        zero = jnp.zeros_like(query)
+        queries[which, :] = jnp.where(first_half, query, zero)
+        queries[pl.ds(pl.multiple_of(count + first, part_rows), part_rows), :] = jnp.where(
+            first_half, zero, query
+        )
+
+    def kv_relay(b):
+        piece = kv_piece(across, b)
+        arrived(piece, kv_ss.at[b, 2], kv_rs.at[b, across])
+        send(None, piece, piece, kv_ss.at[b, 2], kv_rs.at[b, across], twin, t)
+
     for made in qkv_loads:
         made.wait()
     arrived(terms.at[pl.ds(0, T - 1)], term_ss.at[0], term_rs.at[0])
@@ -476,75 +519,62 @@
     kv[pl.ds(i, 1), pl.ds(count, crows), :] = jnp.dot(
         cmod[...], wqkv[:, VALUE:], preferred_element_type=f32
     ).astype(bf16)[None]
-
-    def ckv_piece(s):
-        return kv.at[s, pl.ds(count, crows), :]
-
-    def kv_piece(s):
-        return kv.at[s, pl.ds(0, count), :]
-
     send(None, ckv_piece(i), ckv_piece(i), ckv_ss.at[0], ckv_rs.at[i], across, t)
     send(None, ckv_piece(i), ckv_piece(i), ckv_ss.at[1], ckv_rs.at[i], twin, t)
 
-    def over_view(where, less):
-        return lat.at[pl.ds(0, Z * rows - rows + less), :]
-
-    for where in (outer, inner):
-        def come(where=where):
-            arrived(over_view(where, 0), lat_yss.at[0], lat_yrs.at[0])
-
-        when(where, come)
-    modulate_into(mod, lat, 0, count, 0)
-    projected = jnp.dot(mod[...], wqkv[...], preferred_element_type=f32)
-
-    def rotated(u):
-        turned = jnp.where(even, -pltpu.roll(u, VALUE - quarter, 1), pltpu.roll(u, quarter, 1))
-        return u * tables[0] + turned * tables[1]
-
-    kv[pl.ds(i, 1), pl.ds(0, count), pl.ds(0, VALUE)] = (
-        rotated(projected[:, VALUE : 2 * VALUE]).astype(bf16)[None]
-    )
-    kv[pl.ds(i, 1), pl.ds(0, count), pl.ds(VALUE, VALUE)] = (
-        projected[:, 2 * VALUE :].astype(bf16)[None]
-    )
-    send(None, kv_piece(i), kv_piece(i), kv_ss.at[0], kv_rs.at[i], across, t)
-    send(None, kv_piece(i), kv_piece(i), kv_ss.at[1], kv_rs.at[i], twin, t)
-    query = rotated(projected[:, :VALUE]).astype(bf16) * jnp.asarray(HEAD ** (-0.5), bf16)
-    first_half = lane < HEAD
-    zero = jnp.zeros_like(query)
-    queries[0:count, :] = jnp.where(first_half, query, zero)
-    queries[count:, :] = jnp.where(first_half, zero, query)
-
-    ones = jnp.ones((count + crows, VALUE), bf16)
-
-    def attend(slot):
-        rows_kv = kv[slot]
+    def over_wait(n, ss, rs):
+        view = lat.at[pl.ds(0, n), :]
+        if rs is None:
+            sent_all(view, ss)
+        else:
+            arrived(view, ss, rs)
+
+    over_wait(3 * rows // 2, lat_yss.at[0], lat_yrs.at[0])
+    project_batch(0)
+    lat_stage(3, upper)
+    lat_last()
+    wo_stage(1, inner, True, share=False)
+    when(outer, lambda: over_wait(3 * rows // 2, lat_yss.at[0], lat_yrs.at[1]))
+    when(inner, lambda: over_wait(2 * rows, lat_yss.at[0], lat_yrs.at[1]))
+    project_batch(1)
+    wo_stage(1, inner, True, take=False)
+    wo_stage(2, inner)
+    wo_stage(1, outer)
+    arrived(ckv_piece(across), ckv_ss.at[2], ckv_rs.at[across])
+    send(None, ckv_piece(across), ckv_piece(across), ckv_ss.at[2], ckv_rs.at[across], twin, t)
+    kv_relay(0)
+
+    def attend(rows_kv):
         scores = lax.dot_general(
             queries[...], rows_kv[:, :VALUE], (((1,), (1,)), ((), ())), preferred_element_type=f32
         )
+        ones = jnp.ones((rows_kv.shape[0], VALUE), bf16)
         return jnp.dot(
             jnp.exp(scores).astype(bf16),
             jnp.concatenate([rows_kv[:, VALUE:], ones], axis=1),
             preferred_element_type=f32,
         )
 
-    sums = attend(i)
-    arrived(ckv_piece(across), ckv_ss.at[2], ckv_rs.at[across])
-    send(None, ckv_piece(across), ckv_piece(across), ckv_ss.at[2], ckv_rs.at[across], twin, t)
-    wo_stage(2, inner)
+    def attend_first(s):
+        return attend(jnp.concatenate([kv_piece(s, 0)[...], ckv_piece(s)[...]], axis=0))
+
+    sums = attend(kv[i])
     wo_relay(0)
-    wo_stage(1, outer)
-    arrived(kv_piece(twin), kv_ss.at[2], kv_rs.at[twin])
+    arrived(kv_piece(twin, 0), kv_ss.at[0, 2], kv_rs.at[0, twin])
     arrived(ckv_piece(twin), ckv_ss.at[2], ckv_rs.at[twin])
-    sums = sums + attend(twin)
-    arrived(kv_piece(across), kv_ss.at[2], kv_rs.at[across])
-    send(None, kv_piece(across), kv_piece(across), kv_ss.at[2], kv_rs.at[across], twin, t)
+    sums = sums + attend_first(twin)
+    sums = sums + attend_first(across)
+    arrived(kv_piece(twin_across, 0), kv_ss.at[0, 2], kv_rs.at[0, twin_across])
+    arrived(ckv_piece(twin_across), ckv_ss.at[2], ckv_rs.at[twin_across])
+    sums = sums + attend_first(twin_across)
     wo_stage(1, inner, False)
+    arrived(kv_piece(twin, 1), kv_ss.at[1, 2], kv_rs.at[1, twin])
+    sums = sums + attend(kv_piece(twin, 1)[...])
+    kv_relay(1)
     wo_stage(2, outer)
-    sums = sums + attend(across)
-    arrived(kv_piece(twin_across), kv_ss.at[2], kv_rs.at[twin_across])
-    arrived(ckv_piece(twin_across), ckv_ss.at[2], ckv_rs.at[twin_across])
-    sums = sums + attend(twin_across)
+    sums = sums + attend(kv_piece(across, 1)[...])
+    arrived(kv_piece(twin_across, 1), kv_ss.at[1, 2], kv_rs.at[1, twin_across])
+    sums = sums + attend(kv_piece(twin_across, 1)[...])
     ratio = sums[:, :VALUE] / sums[:, VALUE:]
     difference = ratio[:count] - share_ref[...] * ratio[count:]
     normed = difference * lax.rsqrt(
@@ -562,17 +592,17 @@
 
     wo_stage(3, outer)
     wo_relay(1)
-    wo_relay(2)
-    wo_relay(3)
+    for where in (outer, inner):
+        def second(where=where):
+            if where is outer:
+                wo_relay(2)
+
+        when(where, second)
     drain()
-    for where in (outer, inner):
-        def left(where=where):
-            sent_all(over_view(where, rows // 2), lat_yss.at[0])
-
-        when(where, left)
+    when(outer, lambda: over_wait(7 * rows // 2, lat_yss.at[0], None))
+    when(inner, lambda: over_wait(4 * rows, lat_yss.at[0], None))
     sent_all(part.at[pl.ds(0, S - 1)], part_ss.at[0])
     sent_all(terms.at[pl.ds(0, T - 1)], term_ss.at[0])
-    other_rows = pl.ds(0, (T - 1) * VALUE)
     sent_all(wo_own, wo_mss.at[0])
 
     def wo_sent(heads):
@@ -583,23 +613,47 @@
 
     when(outer, wo_sent(4))
     when(inner, wo_sent(8))
-    arrived(wo.at[other_rows, pl.ds(0, 2 * strip)], wo_tss.at[0], wo_trs.at[0])
+    early_heads = T - 3
+    arrived(wo.at[pl.ds(0, early_heads * VALUE), pl.ds(0, 2 * strip)], wo_tss.at[0], wo_trs.at[0])
     arrived(ho.at[pl.ds(0, T - 1)], ho_ss.at[0], ho_rs.at[0])
-    heads = jnp.concatenate(
-        [
-            jnp.concatenate(
-                [ho[h, pl.ds(pl.multiple_of(which * rows, rows), rows), :] for h in range(T)], axis=1
-            )
-            for which in (1 - y, y)
-        ],
-        axis=0,
-    )
+    span = (T - 2) * VALUE
+    early_head = jnp.where(below, 0, 2)
+    late_first = jnp.where(below, T - 2, 0)
+
+    def heads_of(first, n):
+        return jnp.concatenate(
+            [
+                jnp.concatenate(
+                    [
+                        ho[first + h, pl.ds(pl.multiple_of(which * rows, rows), rows), :]
+                        for h in range(n)
+                    ],
+                    axis=1,
+                )
+                for which in (1 - y, y)
+            ],
+            axis=0,
+        )
+
+    blocks = T // 2
+    heads = heads_of(early_head, T - 2)
+    early_rows = pl.ds(pl.multiple_of(early_head * VALUE, 2 * VALUE), span)
+    for j in range(blocks):
+        acc[:, j * width : (j + 1) * width] = jnp.dot(
+            heads, wo[early_rows, j * width : (j + 1) * width], preferred_element_type=f32
+        )
+    when(inner, lambda: wo_relay(2))
+    wo_relay(3)
+    other_rows = pl.ds(0, (T - 1) * VALUE)
+    arrived(wo.at[pl.ds(0, 2 * VALUE), pl.ds(0, 2 * strip)], wo_tss.at[0], wo_trs.at[1])
+    heads = heads_of(late_first, 2)
+    late_rows = pl.ds(pl.multiple_of(late_first * VALUE, 2 * VALUE), 2 * VALUE)
     near = []
-    blocks = T // 2
     per_piece = blocks // FAR_PIECES
     for j in range(blocks):
-        gated = terms[pl.ds(y * blocks + j, 1), 4:5, :][0] * jnp.dot(
-            heads, wo[:, j * width : (j + 1) * width], preferred_element_type=f32
+        gated = terms[pl.ds(y * blocks + j, 1), 4:5, :][0] * (
+            acc[:, j * width : (j + 1) * width]
+            + jnp.dot(heads, wo[late_rows, j * width : (j + 1) * width], preferred_element_type=f32)
         )
         far_send[:, j * width : (j + 1) * width] = gated[:rows].astype(bf16)
         near.append(gated[rows:])
@@ -653,7 +707,7 @@
             pltpu.VMEM((1, 1), f32),
             pltpu.VMEM((1, VALUE), f32),
             pltpu.VMEM((count, D), bf16),
-            pltpu.VMEM((count, D), bf16),
+            pltpu.VMEM((count // 2, D), bf16),
             pltpu.VMEM((crows, D), bf16),
             pltpu.VMEM((D, 3 * VALUE), bf16),
             pltpu.VMEM((T * VALUE, D // 2), bf16),
@@ -670,10 +724,11 @@
             pltpu.VMEM(shift_weight.shape, bf16),
             pltpu.VMEM((rows, D // 2), bf16),
             pltpu.VMEM((rows, D // 2), bf16),
-            dma((16,)), dma((CHUNKS, 5)), dma((CHUNKS, Z + 1)), dma((CHUNKS,)), dma((1,)), dma((1,)),
+            pltpu.VMEM((2 * rows, D // 2), f32),
+            dma((16,)), dma((CHUNKS, 4)), dma((CHUNKS, Z + 1)), dma((CHUNKS,)), dma((1,)), dma((2,)),
             dma((1,)), dma((1,)), dma((1,)), dma((1,)), pltpu.SemaphoreType.REGULAR((3,)),
-            dma((3,)), dma((S,)), dma((3,)), dma((S,)),
-            dma((1,)), dma((1,)), dma((1,)), dma((1,)), dma((T,)), dma((1,)), dma((T,)), dma((1,)), dma((1,)),
+            dma((2, 3)), dma((2, S)), dma((3,)), dma((S,)),
+            dma((1,)), dma((1,)), dma((1,)), dma((1,)), dma((T,)), dma((1,)), dma((T,)), dma((1,)), dma((2,)),
             dma((FAR_PIECES,)), dma((FAR_PIECES,)),
         ],
         compiler_params=pltpu.CompilerParams(

time: 42.7 us -> 40 us (0.937)
  Pallas kernels: 40.3 us -> 37 us
  local copies, waits for them, and re-layouts: 1.57 us -> 2.01 us
    pallas_call x1, Pallas kernels: 40.3 us -> 37 us  [fused_shards(): pl.pallas_call(functools.partial(fused_kernel, S=S, T=T), out_shape=jax.S...]
    unnamed x1 -> x9, local copies, waits for them, and re-layouts: 1.57 us -> 2.01 us
where the time goes in v2:
time: 40 us; the launch traced here: 39.7 us
  Pallas kernels  37 us (92%)
  local copies, waits for them, and re-layouts  2.01 us (5%)
  between operations  0.69 us (2%)
    pallas_call x1, Pallas kernels, fused_shards(): pl.pallas_call(functools.partial(fused_kernel, S=S, T=T), out_shape=jax.S...  37 us
    unnamed x9, local copies, waits for them, and re-layouts  2.01 us

profile of v2, /device:TPU:0, one launch (start us, length us, event | category | flops | bytes accessed | tf_op | source)
XLA Modules:
  0.0 39.7 jit_solution(17486338998096702637)
XLA Ops:
  0.0 0.0 copy-start
  0.7 0.0 copy-start.1
  0.7 0.0 copy-start.3
  0.7 0.0 copy-done
  0.7 0.7 %copy-done.1 = f32[512]{0:T(512)S(1)} copy-done((f32[512]{0:T(512)S(1)}, f32[512]{0:T(512)}, u32[]{:S(2)}) %copy-start.1) | copy-done | bytes 2072
  1.4 0.0 copy-done.3
  1.4 0.0 copy-start.2
  1.4 0.7 %copy-done.2 = f32[512]{0:T(512)S(1)} copy-done((f32[512]{0:T(512)S(1)}, f32[512]{0:T(512)}, u32[]{:S(2)}) %copy-start.2) | copy-done | bytes 2072
  2.0 37.0 %shard_map.136 = bf16[32,2048]{1,0:T(8,128)(2,1)S(1)} custom-call(bf16[32,2048]{1,0:T(8,128)(2,1)} %lat_hbm.1, bf16[64,2048]{1,0:T(8,128)(2,1)} %ctx_hbm.1, f32[1,512]{1,0:T(1,128)S(1)} %bitcast.7, f32[1,512]{1,0:T(1,128)S(1)} %bitcast.8, f32[1,2048]{1,0:T(1,128)S(1)} %bitcast.6, bf16[512,256]{1,0:T(8,128)(2,1)} %shift_hbm.1, bf16[512,256]{1,0:T(8,128)(2,1)} %scale_hbm.1, ...), custom_call_target="tpu_custom_call" | custom-call | tf_op jit(solution)/shard_map/pallas_call | solution.py:697
  39.0 0.7 %copy.17 = bf16[32,2048]{1,0:T(8,128)(2,1)} copy(bf16[32,2048]{1,0:T(8,128)(2,1)S(1)} %shard_map.136) | data formatting | bytes 262144
Async XLA Ops:
  0.0 0.7 %copy-start = (f32[2048]{0:T(1024)S(1)}, f32[2048]{0:T(1024)}, u32[]{:S(2)}) copy-start(f32[2048]{0:T(1024)} %param.18) | copy-start | bytes 24580
  0.7 0.7 %copy-start.1 = (f32[512]{0:T(512)S(1)}, f32[512]{0:T(512)}, u32[]{:S(2)}) copy-start(f32[512]{0:T(512)} %param.16) | copy-start | bytes 6148
  0.7 0.7 %copy-start.3 = (f32[128]{0:T(128)S(1)}, f32[128]{0:T(128)}, u32[]{:S(2)}) copy-start(f32[128]{0:T(128)} %param.26) | copy-start | bytes 1540
  1.4 0.7 %copy-start.2 = (f32[512]{0:T(512)S(1)}, f32[512]{0:T(512)}, u32[]{:S(2)}) copy-start(f32[512]{0:T(512)} %param.17) | copy-start | bytes 6148

commit v3 on v2

--- a/solution.py
+++ b/solution.py
@@ -453,8 +453,9 @@
     wo_share(None, mate)
     for head in (t, mate):
         wo_launch(None, head, midward)
+    lat_stage(2)
+    for head in (t, mate):
         wo_launch(outer, head, inward)
-    lat_stage(2)
     wo_launch(inner, t, outward)
     wo_launch(inner, mate, outward)
     lat_stage(3, range(CHUNKS // 2))

time: 40 us -> 39.7 us (level)
  no operation moved by 1% of the time
where the time goes in v3:
time: 39.7 us; the launch traced here: 39.4 us
  Pallas kernels  36.7 us (92%)
  local copies, waits for them, and re-layouts  2.01 us (5%)
  between operations  0.69 us (2%)
    pallas_call x1, Pallas kernels, fused_shards(): pl.pallas_call(functools.partial(fused_kernel, S=S, T=T), out_shape=jax.S...  36.7 us
    unnamed x9, local copies, waits for them, and re-layouts  2.01 us

profile of v3, /device:TPU:0, one launch (start us, length us, event | category | flops | bytes accessed | tf_op | source)
XLA Modules:
  0.0 39.4 jit_solution(3189433294393059805)
XLA Ops:
  0.0 0.0 copy-start
  0.7 0.0 copy-start.1
  0.7 0.0 copy-start.3
  0.7 0.0 copy-done
  0.7 0.7 %copy-done.1 = f32[512]{0:T(512)S(1)} copy-done((f32[512]{0:T(512)S(1)}, f32[512]{0:T(512)}, u32[]{:S(2)}) %copy-start.1) | copy-done | bytes 2072
  1.4 0.0 copy-done.3
  1.4 0.0 copy-start.2
  1.4 0.7 %copy-done.2 = f32[512]{0:T(512)S(1)} copy-done((f32[512]{0:T(512)S(1)}, f32[512]{0:T(512)}, u32[]{:S(2)}) %copy-start.2) | copy-done | bytes 2072
  2.0 36.7 %shard_map.136 = bf16[32,2048]{1,0:T(8,128)(2,1)S(1)} custom-call(bf16[32,2048]{1,0:T(8,128)(2,1)} %lat_hbm.1, bf16[64,2048]{1,0:T(8,128)(2,1)} %ctx_hbm.1, f32[1,512]{1,0:T(1,128)S(1)} %bitcast.7, f32[1,512]{1,0:T(1,128)S(1)} %bitcast.8, f32[1,2048]{1,0:T(1,128)S(1)} %bitcast.6, bf16[512,256]{1,0:T(8,128)(2,1)} %shift_hbm.1, bf16[512,256]{1,0:T(8,128)(2,1)} %scale_hbm.1, ...), custom_call_target="tpu_custom_call" | custom-call | tf_op jit(solution)/shard_map/pallas_call | solution.py:698
  38.8 0.7 %copy.17 = bf16[32,2048]{1,0:T(8,128)(2,1)} copy(bf16[32,2048]{1,0:T(8,128)(2,1)S(1)} %shard_map.136) | data formatting | bytes 262144
Async XLA Ops:
  0.0 0.7 %copy-start = (f32[2048]{0:T(1024)S(1)}, f32[2048]{0:T(1024)}, u32[]{:S(2)}) copy-start(f32[2048]{0:T(1024)} %param.18) | copy-start | bytes 24580
  0.7 0.7 %copy-start.1 = (f32[512]{0:T(512)S(1)}, f32[512]{0:T(512)}, u32[]{:S(2)}) copy-start(f32[512]{0:T(512)} %param.16) | copy-start | bytes 6148
  0.7 0.7 %copy-start.3 = (f32[128]{0:T(128)S(1)}, f32[128]{0:T(128)}, u32[]{:S(2)}) copy-start(f32[128]{0:T(128)} %param.26) | copy-start | bytes 1540
  1.4 0.7 %copy-start.2 = (f32[512]{0:T(512)S(1)}, f32[512]{0:T(512)}, u32[]{:S(2)}) copy-start(f32[512]{0:T(512)} %param.17) | copy-start | bytes 6148

commit v4 on v3

--- a/solution.py
+++ b/solution.py
@@ -141,7 +141,7 @@
     lat_hbm, ctx_hbm, cond_hbm, ccond_hbm, gain_hbm, shift_hbm, scale_hbm, gate_hbm,
     wq_hbm, wk_hbm, wv_hbm, share_hbm, hgain_hbm, wo_hbm, out_ref,
     ctx_ref, cond_ref, ccond_ref, gain_ref, share_ref, hgain_ref, lat, mod, cmod, wqkv, wo, wo_own,
-    part, terms, tables, queries, kv, ho_send, ho, shift_ref, scale_ref, gate_ref, far_send, far_recv, acc,
+    part, terms, tables, queries, kv, ho_send, ho, shift_ref, scale_ref, gate_ref, far_send, far_recv, acc, last_heads,
     load_sem, lat_ss, lat_rs, lat_xrs, lat_yss, lat_yrs, part_ss, part_rs, term_ss, term_rs, chain_sem,
     kv_ss, kv_rs, ckv_ss, ckv_rs, ho_ss, ho_rs, wo_mss, wo_ss, wo_rs, wo_xss, wo_xrs, wo_tss, wo_trs,
     far_ss, far_rs,
@@ -538,6 +538,7 @@
     when(outer, lambda: over_wait(3 * rows // 2, lat_yss.at[0], lat_yrs.at[1]))
     when(inner, lambda: over_wait(2 * rows, lat_yss.at[0], lat_yrs.at[1]))
     project_batch(1)
+    wo_stage(1, inner, False)
     wo_stage(1, inner, True, take=False)
     wo_stage(2, inner)
     wo_stage(1, outer)
@@ -568,7 +569,6 @@
     arrived(kv_piece(twin_across, 0), kv_ss.at[0, 2], kv_rs.at[0, twin_across])
     arrived(ckv_piece(twin_across), ckv_ss.at[2], ckv_rs.at[twin_across])
     sums = sums + attend_first(twin_across)
-    wo_stage(1, inner, False)
     arrived(kv_piece(twin, 1), kv_ss.at[1, 2], kv_rs.at[1, twin])
     sums = sums + attend(kv_piece(twin, 1)[...])
     kv_relay(1)
@@ -643,11 +643,12 @@
         acc[:, j * width : (j + 1) * width] = jnp.dot(
             heads, wo[early_rows, j * width : (j + 1) * width], preferred_element_type=f32
         )
+    last_heads[...] = heads_of(late_first, 2)
     when(inner, lambda: wo_relay(2))
     wo_relay(3)
     other_rows = pl.ds(0, (T - 1) * VALUE)
     arrived(wo.at[pl.ds(0, 2 * VALUE), pl.ds(0, 2 * strip)], wo_tss.at[0], wo_trs.at[1])
-    heads = heads_of(late_first, 2)
+    heads = last_heads[...]
     late_rows = pl.ds(pl.multiple_of(late_first * VALUE, 2 * VALUE), 2 * VALUE)
     near = []
     per_piece = blocks // FAR_PIECES
@@ -726,6 +727,7 @@
             pltpu.VMEM((rows, D // 2), bf16),
             pltpu.VMEM((rows, D // 2), bf16),
             pltpu.VMEM((2 * rows, D // 2), f32),
+            pltpu.VMEM((2 * rows, 2 * VALUE), bf16),
             dma((16,)), dma((CHUNKS, 4)), dma((CHUNKS, Z + 1)), dma((CHUNKS,)), dma((1,)), dma((2,)),
             dma((1,)), dma((1,)), dma((1,)), dma((1,)), pltpu.SemaphoreType.REGULAR((3,)),
             dma((2, 3)), dma((2, S)), dma((3,)), dma((S,)),

time: 39.7 us -> 39.6 us (level)
  no operation moved by 1% of the time
where the time goes in v4:
time: 39.6 us; the launch traced here: 39.3 us
  Pallas kernels  36.6 us (92%)
  local copies, waits for them, and re-layouts  2.01 us (5%)
  between operations  0.69 us (2%)
    pallas_call x1, Pallas kernels, fused_shards(): pl.pallas_call(functools.partial(fused_kernel, S=S, T=T), out_shape=jax.S...  36.6 us
    unnamed x9, local copies, waits for them, and re-layouts  2.01 us

profile of v4, /device:TPU:0, one launch (start us, length us, event | category | flops | bytes accessed | tf_op | source)
XLA Modules:
  0.0 39.3 jit_solution(2658868633676177493)
XLA Ops:
  0.0 0.0 copy-start
  0.7 0.0 copy-start.1
  0.7 0.0 copy-start.3
  0.7 0.0 copy-done
  0.7 0.7 %copy-done.1 = f32[512]{0:T(512)S(1)} copy-done((f32[512]{0:T(512)S(1)}, f32[512]{0:T(512)}, u32[]{:S(2)}) %copy-start.1) | copy-done | bytes 2072
  1.4 0.0 copy-done.3
  1.4 0.0 copy-start.2
  1.4 0.7 %copy-done.2 = f32[512]{0:T(512)S(1)} copy-done((f32[512]{0:T(512)S(1)}, f32[512]{0:T(512)}, u32[]{:S(2)}) %copy-start.2) | copy-done | bytes 2072
  2.0 36.6 %shard_map.136 = bf16[32,2048]{1,0:T(8,128)(2,1)S(1)} custom-call(bf16[32,2048]{1,0:T(8,128)(2,1)} %lat_hbm.1, bf16[64,2048]{1,0:T(8,128)(2,1)} %ctx_hbm.1, f32[1,512]{1,0:T(1,128)S(1)} %bitcast.7, f32[1,512]{1,0:T(1,128)S(1)} %bitcast.8, f32[1,2048]{1,0:T(1,128)S(1)} %bitcast.6, bf16[512,256]{1,0:T(8,128)(2,1)} %shift_hbm.1, bf16[512,256]{1,0:T(8,128)(2,1)} %scale_hbm.1, ...), custom_call_target="tpu_custom_call" | custom-call | tf_op jit(solution)/shard_map/pallas_call | solution.py:699
  38.6 0.7 %copy.17 = bf16[32,2048]{1,0:T(8,128)(2,1)} copy(bf16[32,2048]{1,0:T(8,128)(2,1)S(1)} %shard_map.136) | data formatting | bytes 262144
Async XLA Ops:
  0.0 0.7 %copy-start = (f32[2048]{0:T(1024)S(1)}, f32[2048]{0:T(1024)}, u32[]{:S(2)}) copy-start(f32[2048]{0:T(1024)} %param.18) | copy-start | bytes 24580
  0.7 0.7 %copy-start.1 = (f32[512]{0:T(512)S(1)}, f32[512]{0:T(512)}, u32[]{:S(2)}) copy-start(f32[512]{0:T(512)} %param.16) | copy-start | bytes 6148
  0.7 0.7 %copy-start.3 = (f32[128]{0:T(128)S(1)}, f32[128]{0:T(128)}, u32[]{:S(2)}) copy-start(f32[128]{0:T(128)} %param.26) | copy-start | bytes 1540
  1.4 0.7 %copy-start.2 = (f32[512]{0:T(512)S(1)}, f32[512]{0:T(512)}, u32[]{:S(2)}) copy-start(f32[512]{0:T(512)} %param.17) | copy-start | bytes 6148
